TPU v7x, 32 devices: a whole 2x2x4 slice. The times are simulated.
32 devices in a mesh: ep: 8 (over z, x), tp: 4 (over y, core).
Axes of the slice: x: 2, y: 2, z: 4, core: 2. Of those that a mesh axis runs over, the one named last changes fastest.
Arguments:
- tokens: bfloat16 [128, 2048], P('ep'), may hold values from -6 to 6
- norm_attn: float32 [2048], replicated, may hold values from 0.1 to 1.9
- w_query: bfloat16 [2048, 1024], P(None, 'tp'), may hold values from -0.125 to 0.125
- w_key: bfloat16 [2048, 1024], P(None, 'tp'), may hold values from -0.125 to 0.125
- w_value: bfloat16 [2048, 1024], P(None, 'tp'), may hold values from -0.125 to 0.125
- w_forget: bfloat16 [2048, 16], P(None, 'tp'), may hold values from -0.125 to 0.125
- forget_bias: float32 [16], P('tp'), may hold values from -1.5 to 1.5
- w_output: bfloat16 [1024, 2048], P('tp'), may hold values from -0.1875 to 0.1875
- key_cache: bfloat16 [128, 1024, 1024], P('ep', None, 'tp'), may hold values from -488 to 488
- value_cache: bfloat16 [128, 1024, 1024], P('ep', None, 'tp'), may hold values from -6 to 6
- gate_cache: float32 [128, 16, 1024], P('ep', 'tp'), may hold values from -132 to 0, as said below
- lengths: int32 [128], P('ep'), may hold values from 256 to 1024
- norm_ffn: float32 [2048], replicated, may hold values from 0.1 to 1.9
- route_group: int32 [128], P('ep'), may hold values from 0 to 3
- route_slot: int32 [128, 2], P('ep'), may hold values from 0 to 7, as said below
- route_weight: float32 [128, 2], P('ep'), may hold values from 0.2 to 1
- expert_gate: bfloat16 [32, 2048, 1024], P('ep', None, 'tp'), may hold values from -0.125 to 0.125
- expert_up: bfloat16 [32, 2048, 1024], P('ep', None, 'tp'), may hold values from -0.125 to 0.125
- expert_down: bfloat16 [32, 1024, 2048], P('ep', 'tp'), may hold values from -0.1875 to 0.1875
- dense_gate: bfloat16 [2048, 4096], P('tp', 'ep'), may hold values from -0.125 to 0.125
- dense_up: bfloat16 [2048, 4096], P('tp', 'ep'), may hold values from -0.125 to 0.125
- dense_down: bfloat16 [4096, 2048], P('ep', 'tp'), may hold values from -0.09375 to 0.09375
- mix_vector: float32 [2048], replicated, may hold values from -0.125 to 0.125
Outputs:
- mixed_out: bfloat16 [128, 2048], P('ep', 'tp')
Inputs may be any that keep to these rules, and one draw needn't show every extreme that they name: `route_slot`: the two picks of a token are different experts of its group. Among the sequences of one index of ep at most 2 picks name one expert, and in every draw some expert gets exactly 2 picks from every index of ep. `gate_cache`: along the positions of each sequence and head the values never rise.
All inputs are finite; a program needn't handle non-finite values.
Results may differ from a plain program's by a relative error of at most 0.014.
Values may be sent and summed in bfloat16 or wider, within the bound.
A program may use at most 128 MiB of HBM per device.

v0:
```python
import jax
import jax.numpy as jnp
from jax import lax
from jax.sharding import PartitionSpec as P

EXPERTS_PER_GROUP = 8


EPS = 1e-06


def rms_scale(row_block, gain_vector):
    row_block = row_block.astype(jnp.float32)
    return (
        row_block
        * lax.rsqrt(jnp.mean(row_block * row_block, axis=-1, keepdims=True) + EPS)
        * gain_vector
    )


def bf16_round(array):
    return lax.optimization_barrier(array.astype(jnp.bfloat16)).astype(jnp.float32)


def attend(queries, key_new, value_new, forget_log, key_cache, value_cache, gate_cache, lengths):
    seq_count, cache_len, head_width = key_cache.shape
    head_local = gate_cache.shape[1]
    head_size = head_width // head_local
    score_scale = head_size ** (-0.5)
    query_h = queries.reshape(seq_count, head_local, head_size)
    key_rows = key_cache.reshape(seq_count, cache_len, head_local, head_size)
    value_rows = value_cache.reshape(seq_count, cache_len, head_local, head_size)
    entry_indices = jnp.arange(cache_len, dtype=jnp.int32)
    at_last = entry_indices[None, None, :] == (lengths - 1)[:, None, None]
    last_gate = jnp.sum(jnp.where(at_last, gate_cache, jnp.zeros_like(gate_cache)), axis=2)
    current = last_gate + forget_log
    scores = (
        jnp.einsum("shd,sjhd->shj", query_h, key_rows, preferred_element_type=jnp.float32)
        * score_scale
    )
    scores = scores + (current[:, :, None] - gate_cache)
    scores = jnp.where(entry_indices[None, None, :] < lengths[:, None, None], scores, -jnp.inf)
    own_score = (
        jnp.sum(
            query_h.astype(jnp.float32)
            * key_new.reshape(seq_count, head_local, head_size).astype(jnp.float32),
            axis=2,
        )
        * score_scale
    )
    row_peak = jnp.maximum(jnp.max(scores, axis=2), own_score)
    weights = jnp.exp(scores - row_peak[:, :, None])
    own_weight = jnp.exp(own_score - row_peak)
    denominator = jnp.sum(weights, axis=2) + own_weight
    weighted = jnp.einsum(
        "shj,sjhd->shd",
        weights.astype(jnp.bfloat16),
        value_rows,
        preferred_element_type=jnp.float32,
    )
    weighted = weighted + bf16_round(own_weight)[:, :, None] * value_new.reshape(
        seq_count, head_local, head_size
    ).astype(jnp.float32)
    return (weighted / denominator[:, :, None]).astype(jnp.bfloat16).reshape(seq_count, head_width)


def body(
    tokens,
    norm_attn,
    w_query,
    w_key,
    w_value,
    w_forget,
    forget_bias,
    w_output,
    key_cache,
    value_cache,
    gate_cache,
    lengths,
    norm_ffn,
    route_group,
    route_slot,
    route_weight,
    expert_gate,
    expert_up,
    expert_down,
    dense_gate,
    dense_up,
    dense_down,
    mix_vector,
):
    seq_local = tokens.shape[0]
    model_width = tokens.shape[1]
    ep_count = lax.axis_size("ep")
    tp_count = lax.axis_size("tp")
    tp_position = lax.axis_index("tp")
    width_local = model_width // tp_count
    normed = rms_scale(tokens, norm_attn).astype(jnp.bfloat16)
    queries = jnp.dot(normed, w_query, preferred_element_type=jnp.float32).astype(jnp.bfloat16)
    key_new = jnp.dot(normed, w_key, preferred_element_type=jnp.float32).astype(jnp.bfloat16)
    value_new = jnp.dot(normed, w_value, preferred_element_type=jnp.float32).astype(jnp.bfloat16)
    forget_log = jax.nn.log_sigmoid(
        jnp.dot(normed, w_forget, preferred_element_type=jnp.float32) + forget_bias
    )
    attended = attend(
        queries, key_new, value_new, forget_log, key_cache, value_cache, gate_cache, lengths
    )
    head_part = bf16_round(jnp.dot(attended, w_output, preferred_element_type=jnp.float32))
    attn_sum = lax.psum(head_part.astype(jnp.bfloat16), "tp").astype(jnp.float32)
    residual = tokens.astype(jnp.float32) + attn_sum
    normed_ffn = rms_scale(residual, norm_ffn).astype(jnp.bfloat16)
    residual_mine = lax.dynamic_slice_in_dim(residual, tp_position * width_local, width_local, 1)
    normed_mine = lax.dynamic_slice_in_dim(normed_ffn, tp_position * width_local, width_local, 1)
    mix_gate = jax.nn.sigmoid(
        jnp.dot(normed_ffn.astype(jnp.float32), mix_vector, precision=lax.Precision.HIGHEST)
    )
    picks = route_slot.shape[1]
    expert_local = expert_gate.shape[0]
    expert_count = expert_local * ep_count
    capacity = seq_local // EXPERTS_PER_GROUP
    flat_ids = (route_group[:, None] * EXPERTS_PER_GROUP + route_slot).reshape(-1)
    matches = (flat_ids[:, None] == jnp.arange(expert_count, dtype=jnp.int32)[None, :]).astype(
        jnp.int32
    )
    earlier = jnp.sum((jnp.cumsum(matches, axis=0) - matches) * matches, axis=1)
    slot_ids = flat_ids * capacity + earlier
    slot_table = slot_ids[:, None] == jnp.arange(expert_count * capacity, dtype=jnp.int32)[None, :]
    replicas = jnp.repeat(normed_ffn, picks, axis=0)
    outgoing = jnp.einsum(
        "rc,rd->cd", slot_table.astype(jnp.bfloat16), replicas, preferred_element_type=jnp.float32
    ).astype(jnp.bfloat16)
    outgoing = outgoing.reshape(ep_count, expert_local, capacity, model_width)
    arrived = lax.all_to_all(outgoing, "ep", split_axis=0, concat_axis=0, tiled=True)
    gate_act = jnp.einsum(
        "nesd,edf->nesf", arrived, expert_gate, preferred_element_type=jnp.float32
    )
    up_act = jnp.einsum("nesd,edf->nesf", arrived, expert_up, preferred_element_type=jnp.float32)
    hidden = (jax.nn.silu(gate_act) * up_act).astype(jnp.bfloat16)
    partial_value = bf16_round(
        jnp.einsum("nesf,efd->nesd", hidden, expert_down, preferred_element_type=jnp.float32)
    )
    summed = lax.psum_scatter(
        partial_value.astype(jnp.bfloat16), "tp", scatter_dimension=3, tiled=True
    )
    returned = lax.all_to_all(summed, "ep", split_axis=0, concat_axis=0, tiled=True)
    returned = returned.reshape(expert_count * capacity, width_local)
    pick_weights = route_weight.reshape(-1)
    combine_table = jnp.where(slot_table, pick_weights[:, None], jnp.zeros((), jnp.float32))
    combine_table = jnp.sum(
        combine_table.reshape(seq_local, picks, expert_count * capacity), axis=1
    )
    moe = jnp.dot(combine_table, returned.astype(jnp.float32), precision=lax.Precision.HIGHEST)
    hidden_local = dense_gate.shape[1]
    portion = lax.all_gather(normed_mine, "ep", axis=0, tiled=True)
    gate_part = jnp.dot(portion, dense_gate, preferred_element_type=jnp.float32)
    up_part = jnp.dot(portion, dense_up, preferred_element_type=jnp.float32)
    dense_parts = jnp.concatenate([gate_part, up_part], axis=1).astype(jnp.bfloat16)
    dense_pre = lax.psum(dense_parts.astype(jnp.float32).astype(jnp.bfloat16), "tp").astype(
        jnp.float32
    )
    dense_hidden = (jax.nn.silu(dense_pre[:, :hidden_local]) * dense_pre[:, hidden_local:]).astype(
        jnp.bfloat16
    )
    dense_out = lax.psum_scatter(
        jnp.dot(dense_hidden, dense_down, preferred_element_type=jnp.float32).astype(jnp.bfloat16),
        "ep",
        scatter_dimension=0,
        tiled=True,
    ).astype(jnp.float32)
    return (residual_mine + moe + mix_gate[:, None] * dense_out).astype(jnp.bfloat16)


def solution(mesh):
    in_specs = (
        P("ep", None),
        P(),
        P(None, "tp"),
        P(None, "tp"),
        P(None, "tp"),
        P(None, "tp"),
        P("tp"),
        P("tp", None),
        P("ep", None, "tp"),
        P("ep", None, "tp"),
        P("ep", "tp", None),
        P("ep"),
        P(),
        P("ep"),
        P("ep", None),
        P("ep", None),
        P("ep", None, "tp"),
        P("ep", None, "tp"),
        P("ep", "tp", None),
        P("tp", "ep"),
        P("tp", "ep"),
        P("ep", "tp"),
        P(),
    )
    out_specs = P("ep", "tp")
    return jax.shard_map(body, mesh=mesh, in_specs=in_specs, out_specs=out_specs, check_vma=False)
```

profile of v0, /device:TPU:0, one launch (start us, length us, event | category | flops | bytes accessed | tf_op | source)
XLA Modules:
  0.0 254.5 jit_solution(8786818565933185527)
XLA Ops:
  8.0 1.0 fusion.45
  9.0 1.6 convolution_convert_fusion.7
  10.8 12.4 %copy.44 = bf16[16,1024,256]{1,2,0:T(8,128)(2,1)} copy(bf16[16,1024,256]{2,1,0:T(8,128)(2,1)} %param.31) | data formatting | bytes 16777216 | tf_op args[8]
  24.3 4.6 %fusion.72 = f32[16,4,1,1024]{3,2,1,0:T(1,128)S(1)} fusion(bf16[16,4,64,1]{2,3,1,0:T(2,128)(2,1)S(1)} %reshape.153, bf16[16,1024,4,64]{1,3,2,0:T(8,128)(2,1)} %bitcast.84), kind=kOutput, calls=%fused_computation.92 | convolution fusion | flops 8388608 | bytes 8658944 | tf_op jit(solution)/shard_map/shd,sjhd->shj/dot_general | solution.py:38
  29.5 12.4 %copy.47 = bf16[16,1024,256]{1,2,0:T(8,128)(2,1)} copy(bf16[16,1024,256]{2,1,0:T(8,128)(2,1)} %param.32) | data formatting | bytes 16777216 | tf_op args[9]
  42.3 5.7 %fusion.38 = f32[16,4,1,64]{3,2,1,0:T(1,128)S(1)} fusion(bf16[16,1024,4,64]{1,3,2,0:T(8,128)(2,1)} %bitcast.85, bf16[16,4,1024,1]{2,1,0,3:T(4,128)(2,1)S(1)} %get-tuple-element.8), kind=kOutput, calls=%fused_computation.38 | convolution fusion | flops 8388608 | bytes 8536064 | tf_op jit(solution)/shard_map/shj,sjhd->shd/dot_general | solution.py:55
  49.8 33.9 %all-reduce.3.cloned.1.call-done = bf16[16,2048]{1,0:T(8,128)(2,1)} async-done(((bf16[16,2048]{1,0:T(8,128)(2,1)}), bf16[16,2048]{1,0:T(8,128)(2,1)}) %all-reduce.3.cloned.1.call-update) | async-done | bytes 65552 | tf_op jit(solution)/shard_map/psum | solution.py:109
  83.6 1.0 convert_add_fusion
  84.6 0.9 multiply_convert_fusion
  85.6 30.7 %all_gather.3 = bf16[128,512]{1,0:T(8,128)(2,1)S(1)} all-gather(bf16[16,512]{1,0:T(8,128)(2,1)S(1)} %constant_dynamic-slice_fusion), channel_id=1, replica_groups=mesh['ep'=8,'tp'=4] {'ep'}, dimensions={0}, use_global_device_ids=true | all-gather | bytes 147456 | tf_op jit(solution)/shard_map/all_gather | solution.py:154
  116.7 0.9 reshape.139
  117.6 5.4 %all-to-all-start = ((bf16[8,4,2,2048]{3,2,1,0:T(2,128)(2,1)}), bf16[8,4,2,2048]{3,2,1,0:T(2,128)(2,1)S(1)}, u32[]{:S(2)}, u32[]{:S(2)}) async-start(bf16[8,4,2,2048]{3,2,1,0:T(2,128)(2,1)} %reshape.139), calls=%async_computation | async-start | bytes 524288 | tf_op jit(solution)/shard_map/all_to_all | solution.py:133
  124.3 6.9 %all-to-all-done = bf16[8,4,2,2048]{3,2,1,0:T(2,128)(2,1)S(1)} async-done(((bf16[8,4,2,2048]{3,2,1,0:T(2,128)(2,1)}), bf16[8,4,2,2048]{3,2,1,0:T(2,128)(2,1)S(1)}, u32[]{:S(2)}, u32[]{:S(2)}) %all-to-all-start) | async-done | bytes 262176 | tf_op jit(solution)/shard_map/all_to_all | solution.py:133
  131.2 2.9 %fusion.12 = f32[8,4,2,256]{3,0,2,1:T(8,128)S(1)} fusion(bf16[4,2048,256]{2,1,0:T(8,128)(2,1)} %param.39, bf16[8,4,2,2048]{3,2,1,0:T(2,128)(2,1)S(1)} %all-to-all-done), kind=kOutput, calls=%fused_computation.13 | convolution fusion | flops 67108864 | bytes 4521984 | tf_op jit(solution)/shard_map/nesd,edf->nesf/dot_general | solution.py:134
  134.1 5.4 %fusion.9 = bf16[8,4,2,2048]{3,0,2,1:T(8,128)(2,1)} fusion(bf16[4,256,2048]{2,1,0:T(8,128)(2,1)} %param.41, bf16[4,2048,256]{2,1,0:T(8,128)(2,1)} %param.40, bf16[8,4,2,2048]{3,2,1,0:T(2,128)(2,1)S(1)} %all-to-all-done, f32[8,4,2,256]{3,0,2,1:T(8,128)S(1)} %fusion.12), kind=kOutput, calls=%fused_computation.8 | convolution fusion | flops 134447104 | bytes 8978432 | tf_op jit(solution)/shard_map/nesf,efd->nesd/dot_general | solution.py:140
  139.8 19.1 %all-reduce.5.cloned.1.call-done = bf16[128,1024]{1,0:T(8,128)(2,1)} async-done(((bf16[128,1024]{1,0:T(8,128)(2,1)}), bf16[128,1024]{1,0:T(8,128)(2,1)}) %all-reduce.5.cloned.1.call-update) | async-done | bytes 262160 | tf_op jit(solution)/shard_map/psum | solution.py:158
  158.9 1.0 convert_element_type.114
  159.9 0.9 convolution_convert_fusion.2
  160.9 20.5 %reduce-scatter.3.cloned.1.call-done = bf16[8,4,2,512]{3,0,2,1:T(8,128)(2,1)} async-done(((bf16[8,4,2,2048]{3,0,2,1:T(8,128)(2,1)}), bf16[8,4,2,512]{3,0,2,1:T(8,128)(2,1)}) %reduce-scatter.3.cloned.1.call-update) | async-done | bytes 65552 | tf_op jit(solution)/shard_map/reduce_scatter | solution.py:142
  181.5 1.5 copy.52
  183.0 5.5 %all-to-all-start.1 = ((bf16[8,4,2,512]{3,2,1,0:T(2,128)(2,1)}), bf16[8,4,2,512]{3,2,1,0:T(2,128)(2,1)S(1)}, u32[]{:S(2)}, u32[]{:S(2)}) async-start(bf16[8,4,2,512]{3,2,1,0:T(2,128)(2,1)} %copy.52), calls=%async_computation.2 | async-start | bytes 131072 | tf_op jit(solution)/shard_map/all_to_all | solution.py:145
  188.6 6.8 %all-to-all-done.1 = bf16[8,4,2,512]{3,2,1,0:T(2,128)(2,1)S(1)} async-done(((bf16[8,4,2,512]{3,2,1,0:T(2,128)(2,1)}), bf16[8,4,2,512]{3,2,1,0:T(2,128)(2,1)S(1)}, u32[]{:S(2)}, u32[]{:S(2)}) %all-to-all-start.1) | async-done | bytes 65568 | tf_op jit(solution)/shard_map/all_to_all | solution.py:145
  195.4 51.0 %reduce-scatter.5.cloned.1.call-done = bf16[16,512]{1,0:T(8,128)(2,1)} async-done(((bf16[128,512]{1,0:T(8,128)(2,1)}), bf16[16,512]{1,0:T(8,128)(2,1)}) %reduce-scatter.5.cloned.1.call-update) | async-done | bytes 16400 | tf_op jit(solution)/shard_map/reduce_scatter | solution.py:164
  246.5 1.5 fusion.25
  (85 shorter events, 7.8 us)
Async XLA Ops:
  6.5 41.7 %copy-start = (bf16[256,2048]{1,0:T(8,128)(2,1)S(1)}, bf16[256,2048]{1,0:T(8,128)(2,1)}, u32[]{:S(2)}) copy-start(bf16[256,2048]{1,0:T(8,128)(2,1)} %param.30) | copy-start | bytes 3145732
  6.5 77.1 %all-reduce.3.cloned.1.call-start = ((), (), s32[]{:S(2)}) async-start(), calls=%async_computation.4 | async-start | bytes 131072 | tf_op jit(solution)/shard_map/psum | solution.py:109
  10.8 12.5 %copy-start.2 = (f32[16,4,1024]{2,1,0:T(4,128)S(1)}, f32[16,4,1024]{2,1,0:T(4,128)}, u32[]{:S(2)}) copy-start(f32[16,4,1024]{2,1,0:T(4,128)} %param.33) | copy-start | bytes 786436
  10.8 12.8 %copy-start.1 = (bf16[16,2048]{1,0:T(8,128)(2,1)S(1)}, bf16[16,2048]{1,0:T(8,128)(2,1)}, u32[]{:S(2)}) copy-start(bf16[16,2048]{1,0:T(8,128)(2,1)} %param.23) | copy-start | bytes 196612
  10.8 12.8 %copy-start.7 = (f32[2048]{0:T(1024)S(1)}, f32[2048]{0:T(1024)}, u32[]{:S(2)}) copy-start(f32[2048]{0:T(1024)} %param.24) | copy-start | bytes 24580
  10.8 12.8 %copy-start.12 = (bf16[2048,4]{0,1:T(4,128)(2,1)S(1)}, bf16[2048,4]{0,1:T(4,128)(2,1)}, u32[]{:S(2)}) copy-start(bf16[2048,4]{0,1:T(4,128)(2,1)} %param.28) | copy-start | bytes 49156
  10.8 12.8 %copy-start.14 = (f32[4]{0:T(128)S(1)}, f32[4]{0:T(128)}, u32[]{:S(2)}) copy-start(f32[4]{0:T(128)} %param.29) | copy-start | bytes 52
  10.8 13.1 %copy-start.3 = (bf16[2048,256]{1,0:T(8,128)(2,1)S(1)}, bf16[2048,256]{1,0:T(8,128)(2,1)}, u32[]{:S(2)}) copy-start(bf16[2048,256]{1,0:T(8,128)(2,1)} %param.26) | copy-start | bytes 3145732
  29.5 12.4 %copy-start.4 = (bf16[2048,256]{1,0:T(8,128)(2,1)S(1)}, bf16[2048,256]{1,0:T(8,128)(2,1)}, u32[]{:S(2)}) copy-start(bf16[2048,256]{1,0:T(8,128)(2,1)} %param.27) | copy-start | bytes 3145732
  42.3 6.9 %copy-start.9 = (s32[16,2]{0,1:T(2,128)S(1)}, s32[16,2]{0,1:T(2,128)}, u32[]{:S(2)}) copy-start(s32[16,2]{0,1:T(2,128)} %param.37) | copy-start | bytes 388
  42.3 7.0 %copy-start.15 = (s32[16]{0:T(128)S(1)}, s32[16]{0:T(128)}, u32[]{:S(2)}) copy-start(s32[16]{0:T(128)} %param.36) | copy-start | bytes 196
  42.3 42.3 %copy-start.8 = (f32[2048]{0:T(1024)S(1)}, f32[2048]{0:T(1024)}, u32[]{:S(2)}) copy-start(f32[2048]{0:T(1024)} %param.35) | copy-start | bytes 24580
  42.3 80.7 %copy-start.5 = (bf16[512,512]{1,0:T(8,128)(2,1)S(1)}, bf16[512,512]{1,0:T(8,128)(2,1)}, u32[]{:S(2)}) copy-start(bf16[512,512]{1,0:T(8,128)(2,1)} %param.43) | copy-start | bytes 1572868
  48.1 75.2 %copy-start.6 = (bf16[512,512]{1,0:T(8,128)(2,1)S(1)}, bf16[512,512]{1,0:T(8,128)(2,1)}, u32[]{:S(2)}) copy-start(bf16[512,512]{1,0:T(8,128)(2,1)} %param.42) | copy-start | bytes 1572868
  117.6 13.6 %all-to-all-start = ((bf16[8,4,2,2048]{3,2,1,0:T(2,128)(2,1)}), bf16[8,4,2,2048]{3,2,1,0:T(2,128)(2,1)S(1)}, u32[]{:S(2)}, u32[]{:S(2)}) async-start(bf16[8,4,2,2048]{3,2,1,0:T(2,128)(2,1)} %reshape.139), calls=%async_computation | async-start | bytes 524288 | tf_op jit(solution)/shard_map/all_to_all | solution.py:133
  122.9 36.0 %all-reduce.5.cloned.1.call-start = ((), (), s32[]{:S(2)}) async-start(), calls=%async_computation.6 | async-start | bytes 524288 | tf_op jit(solution)/shard_map/psum | solution.py:158
  124.2 57.2 %reduce-scatter.3.cloned.1.call-start = ((), (), s32[]{:S(2)}) async-start(), calls=%async_computation.5 | async-start | bytes 327680 | tf_op jit(solution)/shard_map/reduce_scatter | solution.py:142
  134.0 25.9 %copy-start.11 = (bf16[512,512]{1,0:T(8,128)(2,1)S(1)}, bf16[512,512]{1,0:T(8,128)(2,1)}, u32[]{:S(2)}) copy-start(bf16[512,512]{1,0:T(8,128)(2,1)} %param.44) | copy-start | bytes 1572868
  134.0 26.8 %copy-start.10 = (f32[16,2]{0,1:T(2,128)S(1)}, f32[16,2]{0,1:T(2,128)}, u32[]{:S(2)}) copy-start(f32[16,2]{0,1:T(2,128)} %param.38) | copy-start | bytes 388
  134.0 54.4 %copy-start.13 = (f32[2048]{0:T(1024)S(1)}, f32[2048]{0:T(1024)}, u32[]{:S(2)}) copy-start(f32[2048]{0:T(1024)} %param.45) | copy-start | bytes 24580
  139.5 106.9 %reduce-scatter.5.cloned.1.call-start = ((), (), s32[]{:S(2)}) async-start(), calls=%async_computation.7 | async-start | bytes 147456 | tf_op jit(solution)/shard_map/reduce_scatter | solution.py:164
  183.0 12.4 %all-to-all-start.1 = ((bf16[8,4,2,512]{3,2,1,0:T(2,128)(2,1)}), bf16[8,4,2,512]{3,2,1,0:T(2,128)(2,1)S(1)}, u32[]{:S(2)}, u32[]{:S(2)}) async-start(bf16[8,4,2,512]{3,2,1,0:T(2,128)(2,1)} %copy.52), calls=%async_computation.2 | async-start | bytes 131072 | tf_op jit(solution)/shard_map/all_to_all | solution.py:145
Sparse Core Ops, SparseCore 0:
  49.3 34.2 all-reduce.2
  126.1 32.7 all-reduce.4
  161.4 20.0 reduce-scatter.2
  184.6 61.7 reduce-scatter.4
where the time goes:
time: 256 us; the launch traced here: 254 us
  waiting for transfers between devices  138 us (54%)
  blocking collectives  30.7 us (12%)
  local copies, waits for them, and re-layouts  28.3 us (11%)
  matrix products  25.1 us (10%)
  between operations  13.4 us (5%)
  starting transfers between devices  11 us (4%)
  other arithmetic  7.66 us (3%)
    reduce_scatter x1, waiting for transfers between devices, body(): lax.psum_scatter(jnp.dot(dense_hidden, dense_down, preferred_element_type...  51 us
    psum x1, waiting for transfers between devices, body(): lax.psum(head_part.astype(jnp.bfloat16), 'tp').astype(jnp.float32)  33.9 us
    all_gather x1, blocking collectives, body(): portion = lax.all_gather(normed_mine, 'ep', axis=0, tiled=True)  30.7 us
    unnamed x35, local copies, waits for them, and re-layouts  24.9 us
    reduce_scatter x1, waiting for transfers between devices, body(): lax.psum_scatter(partial_value.astype(jnp.bfloat16), 'tp', scatter_dimens...  20.5 us
    psum x1, waiting for transfers between devices, body(): lax.psum(dense_parts.astype(jnp.float32).astype(jnp.bfloat16), 'tp')  19.1 us
    all_to_all x1, waiting for transfers between devices, body(): lax.all_to_all(outgoing, 'ep', split_axis=0, concat_axis=0, tiled=True)  6.88 us
    all_to_all x1, waiting for transfers between devices, body(): lax.all_to_all(summed, 'ep', split_axis=0, concat_axis=0, tiled=True)  6.78 us
  transfers between devices with their start and end apart: 6, of which 6 were waited for; matrix products, arithmetic and copies ran while one was open for 5% of the time, Pallas kernels for 0%

commit v1 on v0

v1 whole, which is shorter than its diff:
```python
import functools

import jax
import jax.numpy as jnp
from jax import lax
from jax.experimental import pallas as pl
from jax.experimental.pallas import tpu as pltpu
from jax.sharding import PartitionSpec as P

EXPERTS_PER_GROUP = 8


EPS = 1e-06
F32 = jnp.float32
BF16 = jnp.bfloat16
MESH = pl.DeviceIdType.MESH
VMEM = pl.BlockSpec(memory_space=pltpu.VMEM)
NT = (((1,), (1,)), ((), ()))


def rms_scale(row_block, gain):
    return row_block * lax.rsqrt(jnp.mean(row_block * row_block, axis=-1, keepdims=True) + EPS) * gain


def attend_kernel(
    batch, len_ref, tok_ref, gain_ref, wq_ref, wk_ref, wv_ref, wf_ref, bias_ref, wo_ref,
    key_ref, value_ref, gate_ref, out_ref, q_scr, k_scr, v_scr, f_scr, a_scr,
):
    step = pl.program_id(0)
    heads = wf_ref.shape[0]
    width = wq_ref.shape[1]
    cache_len = key_ref.shape[1]
    head_size = width // heads
    score_scale = head_size ** (-0.5)

    @pl.when(step == 0)
    def _():
        normed = rms_scale(tok_ref[...].astype(F32), gain_ref[...]).astype(BF16)
        for w_ref, scr in ((wq_ref, q_scr), (wk_ref, k_scr), (wv_ref, v_scr)):
            made = jnp.dot(normed, w_ref[...], preferred_element_type=F32)
            scr[...] = made.astype(BF16).astype(F32)
        logit = lax.dot_general(wf_ref[...], normed, NT, preferred_element_type=F32)
        f_scr[...] = jax.nn.log_sigmoid(logit + bias_ref[...])

    head_of = lax.broadcasted_iota(jnp.int32, (heads, width), 1) // head_size
    mine = head_of == lax.broadcasted_iota(jnp.int32, (heads, width), 0)
    position = lax.broadcasted_iota(jnp.int32, (heads, cache_len), 1)
    seq_lane = lax.broadcasted_iota(jnp.int32, f_scr.shape, 1)
    for i in range(batch):
        s = step * batch + i
        length = len_ref[s]
        query = q_scr[pl.ds(s, 1), :]
        query_heads = jnp.where(mine, query, 0.0)
        gate = gate_ref[i]
        forget = jnp.sum(jnp.where(seq_lane == s, f_scr[...], 0.0), axis=1, keepdims=True)
        last = jnp.sum(jnp.where(position == length - 1, gate, 0.0), axis=1, keepdims=True)
        scores = lax.dot_general(
            query_heads.astype(BF16), key_ref[i], NT, preferred_element_type=F32
        ) * score_scale
        scores = scores + ((last + forget) - gate)
        scores = jnp.where(position < length, scores, -jnp.inf)
        own = jnp.sum(query_heads * k_scr[pl.ds(s, 1), :], axis=1, keepdims=True) * score_scale
        peak = jnp.maximum(jnp.max(scores, axis=1, keepdims=True), own)
        weights = jnp.exp(scores - peak)
        own_weight = jnp.exp(own - peak)
        denominator = jnp.sum(weights, axis=1, keepdims=True) + own_weight
        weighted = jnp.dot(weights.astype(BF16), value_ref[i], preferred_element_type=F32)
        weighted = weighted + own_weight.astype(BF16).astype(F32) * v_scr[pl.ds(s, 1), :]
        result = jnp.where(mine, weighted / denominator, 0.0)
        a_scr[pl.ds(s, 1), :] = jnp.sum(result, axis=0, keepdims=True)

    @pl.when(step == pl.num_programs(0) - 1)
    def _():
        out_ref[...] = jnp.dot(
            a_scr[...].astype(BF16), wo_ref[...], preferred_element_type=F32
        ).astype(BF16)


def attention(tokens, gain, wq, wk, wv, wf, bias, wo, key_cache, value_cache, gate_cache, lengths):
    seqs, model = tokens.shape
    _, cache_len, width = key_cache.shape
    heads = gate_cache.shape[1]
    batch = 4 if seqs % 4 == 0 else 1
    whole = lambda shape: pl.BlockSpec(shape, lambda i: (0,) * len(shape))
    return pl.pallas_call(
        functools.partial(attend_kernel, batch),
        grid=(seqs // batch,),
        out_shape=jax.ShapeDtypeStruct((seqs, model), BF16),
        in_specs=[
            pl.BlockSpec(memory_space=pltpu.SMEM),
            whole((seqs, model)),
            whole((1, model)),
            whole(wq.shape),
            whole(wk.shape),
            whole(wv.shape),
            whole((heads, model)),
            whole((heads, 1)),
            whole(wo.shape),
            pl.BlockSpec((batch, cache_len, width), lambda i: (i, 0, 0)),
            pl.BlockSpec((batch, cache_len, width), lambda i: (i, 0, 0)),
            pl.BlockSpec((batch, heads, cache_len), lambda i: (i, 0, 0)),
        ],
        out_specs=whole((seqs, model)),
        scratch_shapes=[
            pltpu.VMEM((seqs, width), F32),
            pltpu.VMEM((seqs, width), F32),
            pltpu.VMEM((seqs, width), F32),
            pltpu.VMEM((heads, seqs), F32),
            pltpu.VMEM((seqs, width), F32),
        ],
        compiler_params=pltpu.CompilerParams(
            dimension_semantics=("arbitrary",), vmem_limit_bytes=48 * 1024 * 1024
        ),
        name="attend",
    )(
        lengths, tokens, gain[None, :], wq, wk, wv, wf.T, bias[:, None], wo,
        key_cache, value_cache, gate_cache,
    )


def greet(axis, count):
    me = lax.axis_index(axis)
    barrier = pltpu.get_barrier_semaphore()
    for k in range(1, count):
        pl.semaphore_signal(
            barrier, inc=1, device_id={axis: lax.rem(me + k, count)}, device_id_type=MESH
        )
    pl.semaphore_wait(barrier, count - 1)
    return me


def remote(axis, peer, src, dst, send, recv):
    copy = pltpu.make_async_remote_copy(
        src_ref=src, dst_ref=dst, send_sem=send, recv_sem=recv,
        device_id={axis: peer}, device_id_type=MESH,
    )
    copy.start()
    return copy


def comm_params(number):
    return pltpu.CompilerParams(
        collective_id=number, has_side_effects=True, vmem_limit_bytes=32 * 1024 * 1024
    )


def residual_kernel(
    count, part_ref, tok_ref, gain_ref, table_ref, res_ref, norm_ref, out_ref, land, send, recv
):
    me = greet("tp", count)
    copies = [
        remote("tp", lax.rem(me + k, count), part_ref, land.at[k - 1], send.at[k - 1], recv.at[k - 1])
        for k in range(1, count)
    ]
    total = part_ref[...].astype(F32)
    for k in range(1, count):
        copies[k - 1].wait_recv()
        total = total + land[k - 1].astype(F32)
    residual = tok_ref[...].astype(F32) + total
    res_ref[...] = residual
    normed = rms_scale(residual, gain_ref[...]).astype(BF16)
    norm_ref[...] = normed
    out_ref[...] = jnp.dot(table_ref[...], normed, preferred_element_type=F32).astype(BF16)
    for copy in copies:
        copy.wait_send()


def spread_kernel(count, tp_count, rows_ref, norm_ref, arr_ref, por_ref, land_a, land_p, sems):
    me = greet("ep", count)
    width = por_ref.shape[2]
    own_cols = pl.ds(pl.multiple_of(lax.axis_index("tp") * width, width), width)
    copies = []
    for k in range(1, count):
        peer = lax.rem(me + k, count)
        copies.append(
            remote("ep", peer, norm_ref.at[:, own_cols], land_p.at[k - 1], sems.at[0, k - 1], sems.at[1, k - 1])
        )
        copies.append(
            remote("ep", peer, rows_ref.at[peer], land_a.at[k - 1], sems.at[2, k - 1], sems.at[3, k - 1])
        )
    por_ref[me] = norm_ref[:, own_cols]
    arr_ref[me] = rows_ref[me]
    for k in range(1, count):
        source = lax.rem(me + count - k, count)
        copies[2 * k - 2].wait_recv()
        por_ref[source] = land_p[k - 1]
        copies[2 * k - 1].wait_recv()
        arr_ref[source] = land_a[k - 1]
    for copy in copies:
        copy.wait_send()


def reduce_kernel(
    count, gate_ref, up_ref, moe_ref, hid_ref, sum_ref, land_g, land_u, land_m, hidden, sems
):
    me = greet("tp", count)
    width = sum_ref.shape[1]
    columns = lambda peer: pl.ds(pl.multiple_of(peer * width, width), width)
    dense, moes = [], []
    for k in range(1, count):
        peer = lax.rem(me + k, count)
        for order, (ref, land) in enumerate(((gate_ref, land_g), (up_ref, land_u))):
            dense.append(
                remote("tp", peer, ref.at[peer], land.at[k - 1], sems.at[2 * order, k - 1], sems.at[2 * order + 1, k - 1])
            )
    for k in range(1, count):
        peer = lax.rem(me + k, count)
        moes.append(
            remote("tp", peer, moe_ref.at[:, columns(peer)], land_m.at[k - 1], sems.at[4, k - 1], sems.at[5, k - 1])
        )
    gate_sum = gate_ref[me].astype(F32)
    up_sum = up_ref[me].astype(F32)
    for k in range(1, count):
        dense[2 * k - 2].wait_recv()
        dense[2 * k - 1].wait_recv()
        gate_sum = gate_sum + land_g[k - 1].astype(F32)
        up_sum = up_sum + land_u[k - 1].astype(F32)
    hidden[me] = (jax.nn.silu(gate_sum) * up_sum).astype(BF16)
    finals = []
    for k in range(1, count):
        peer = lax.rem(me + k, count)
        finals.append(
            remote("tp", peer, hidden.at[me], hidden.at[me], sems.at[6, k - 1], sems.at[7, k - 1])
        )
    total = moe_ref[:, columns(me)].astype(F32)
    for k in range(1, count):
        moes[k - 1].wait_recv()
        total = total + land_m[k - 1].astype(F32)
    sum_ref[...] = total.astype(BF16)
    for copy in finals:
        copy.wait_recv()
    hid_ref[...] = hidden[...]
    for copy in dense + moes + finals:
        copy.wait_send()


def gather_kernel(count, dense_ref, moe_ref, out_ref, ret_ref, land_d, land_m, sems):
    me = greet("ep", count)
    copies = []
    for k in range(1, count):
        peer = lax.rem(me + k, count)
        copies.append(
            remote("ep", peer, dense_ref.at[peer], land_d.at[k - 1], sems.at[0, k - 1], sems.at[1, k - 1])
        )
        copies.append(
            remote("ep", peer, moe_ref.at[peer], land_m.at[k - 1], sems.at[2, k - 1], sems.at[3, k - 1])
        )
    total = dense_ref[me].astype(F32)
    ret_ref[me] = moe_ref[me]
    for k in range(1, count):
        copies[2 * k - 2].wait_recv()
        total = total + land_d[k - 1].astype(F32)
        copies[2 * k - 1].wait_recv()
        ret_ref[lax.rem(me + count - k, count)] = land_m[k - 1]
    out_ref[...] = total
    for copy in copies:
        copy.wait_send()


def call_comm(kernel, number, ins, outs, scratch):
    return pl.pallas_call(
        kernel,
        out_shape=[jax.ShapeDtypeStruct(shape, dtype) for shape, dtype in outs],
        in_specs=[VMEM] * len(ins),
        out_specs=[VMEM] * len(outs),
        scratch_shapes=scratch,
        compiler_params=comm_params(number),
        name=f"comm_{number}",
    )(*ins)


def body(
    tokens,
    norm_attn,
    w_query,
    w_key,
    w_value,
    w_forget,
    forget_bias,
    w_output,
    key_cache,
    value_cache,
    gate_cache,
    lengths,
    norm_ffn,
    route_group,
    route_slot,
    route_weight,
    expert_gate,
    expert_up,
    expert_down,
    dense_gate,
    dense_up,
    dense_down,
    mix_vector,
):
    seqs, model = tokens.shape
    ep_count = lax.axis_size("ep")
    tp_count = lax.axis_size("tp")
    tp_position = lax.axis_index("tp")
    width = model // tp_count
    picks = route_slot.shape[1]
    expert_local = expert_gate.shape[0]
    expert_count = expert_local * ep_count
    capacity = seqs // EXPERTS_PER_GROUP
    slots = expert_local * capacity
    dma = pltpu.SemaphoreType.DMA

    flat_ids = (route_group[:, None] * EXPERTS_PER_GROUP + route_slot).reshape(-1)
    matches = flat_ids[:, None] == flat_ids[None, :]
    before = jnp.arange(seqs * picks)[None, :] < jnp.arange(seqs * picks)[:, None]
    earlier = jnp.sum((matches & before).astype(jnp.int32), axis=1)
    slot_ids = (flat_ids * capacity + earlier).reshape(seqs, picks)
    all_slots = jnp.arange(expert_count * capacity, dtype=jnp.int32)
    hits = slot_ids[:, :, None] == all_slots[None, None, :]
    send_table = jnp.any(slot_ids[None, :, :] == all_slots[:, None, None], axis=2).astype(BF16)
    combine_table = jnp.sum(jnp.where(hits, route_weight[:, :, None], 0.0), axis=1)

    head_part = attention(
        tokens, norm_attn, w_query, w_key, w_value, w_forget, forget_bias, w_output,
        key_cache, value_cache, gate_cache, lengths,
    )
    residual, normed_ffn, outgoing = call_comm(
        functools.partial(residual_kernel, tp_count),
        1,
        (head_part, tokens, norm_ffn[None, :], send_table),
        (((seqs, model), F32), ((seqs, model), BF16), ((expert_count * capacity, model), BF16)),
        [pltpu.VMEM((tp_count - 1, seqs, model), BF16), dma((tp_count - 1,)), dma((tp_count - 1,))],
    )
    arrived, portion = call_comm(
        functools.partial(spread_kernel, ep_count, tp_count),
        2,
        (outgoing.reshape(ep_count, slots, model), normed_ffn),
        (((ep_count, slots, model), BF16), ((ep_count, seqs, width), BF16)),
        [
            pltpu.VMEM((ep_count - 1, slots, model), BF16),
            pltpu.VMEM((ep_count - 1, seqs, width), BF16),
            dma((4, ep_count - 1)),
        ],
    )
    portion = portion.reshape(ep_count * seqs, width)
    hidden_local = dense_gate.shape[1]
    tokens_all = ep_count * seqs
    gate_part = jnp.dot(portion, dense_gate, preferred_element_type=F32).astype(BF16)
    up_part = jnp.dot(portion, dense_up, preferred_element_type=F32).astype(BF16)

    arrived = arrived.reshape(ep_count, expert_local, capacity, model)
    gate_act = jnp.einsum("nesd,edf->nesf", arrived, expert_gate, preferred_element_type=F32)
    up_act = jnp.einsum("nesd,edf->nesf", arrived, expert_up, preferred_element_type=F32)
    hidden = (jax.nn.silu(gate_act) * up_act).astype(BF16)
    partial_value = jnp.einsum(
        "nesf,efd->nesd", hidden, expert_down, preferred_element_type=F32
    ).astype(BF16)

    row_part = tokens_all // tp_count
    dense_hidden, summed = call_comm(
        functools.partial(reduce_kernel, tp_count),
        3,
        (
            gate_part.reshape(tp_count, row_part, hidden_local),
            up_part.reshape(tp_count, row_part, hidden_local),
            partial_value.reshape(ep_count * slots, model),
        ),
        (((tp_count, row_part, hidden_local), BF16), ((ep_count * slots, width), BF16)),
        [
            pltpu.VMEM((tp_count - 1, row_part, hidden_local), BF16),
            pltpu.VMEM((tp_count - 1, row_part, hidden_local), BF16),
            pltpu.VMEM((tp_count - 1, ep_count * slots, width), BF16),
            pltpu.VMEM((tp_count, row_part, hidden_local), BF16),
            dma((8, tp_count - 1)),
        ],
    )
    dense_part = jnp.dot(
        dense_hidden.reshape(tokens_all, hidden_local), dense_down, preferred_element_type=F32
    ).astype(BF16)
    dense_out, returned = call_comm(
        functools.partial(gather_kernel, ep_count),
        4,
        (dense_part.reshape(ep_count, seqs, width), summed.reshape(ep_count, slots, width)),
        (((seqs, width), F32), ((ep_count, slots, width), BF16)),
        [
            pltpu.VMEM((ep_count - 1, seqs, width), BF16),
            pltpu.VMEM((ep_count - 1, slots, width), BF16),
            dma((4, ep_count - 1)),
        ],
    )
    returned = returned.reshape(expert_count * capacity, width)
    moe = jnp.dot(combine_table, returned.astype(F32), precision=lax.Precision.HIGHEST)
    mix_gate = jax.nn.sigmoid(
        jnp.dot(normed_ffn.astype(F32), mix_vector, precision=lax.Precision.HIGHEST)
    )
    residual_mine = lax.dynamic_slice_in_dim(residual, tp_position * width, width, 1)
    return (residual_mine + moe + mix_gate[:, None] * dense_out).astype(BF16)


def solution(mesh):
    in_specs = (
        P("ep", None),
        P(),
        P(None, "tp"),
        P(None, "tp"),
        P(None, "tp"),
        P(None, "tp"),
        P("tp"),
        P("tp", None),
        P("ep", None, "tp"),
        P("ep", None, "tp"),
        P("ep", "tp", None),
        P("ep"),
        P(),
        P("ep"),
        P("ep", None),
        P("ep", None),
        P("ep", None, "tp"),
        P("ep", None, "tp"),
        P("ep", "tp", None),
        P("tp", "ep"),
        P("tp", "ep"),
        P("ep", "tp"),
        P(),
    )
    out_specs = P("ep", "tp")
    return jax.shard_map(body, mesh=mesh, in_specs=in_specs, out_specs=out_specs, check_vma=False)
```

time: 256 us -> 70.7 us (0.28)
  waiting for transfers between devices: 138 us -> 0 us
  Pallas kernels: 0 us -> 50.6 us
  blocking collectives: 30.7 us -> 0 us
  matrix products: 25.1 us -> 6.97 us
  local copies, waits for them, and re-layouts: 28.3 us -> 11.2 us
  between operations: 13.4 us -> 0.18 us
  starting transfers between devices: 11 us -> 0 us
  other arithmetic: 7.66 us -> 1.2 us
    reduce_scatter x2 -> x0, waiting for transfers between devices: 71.6 us -> none  [the longest x1 51 us: body(): lax.psum_scatter(jnp.dot(dense_hidden, dense_down, preferred_element_type...]
    psum x2 -> x0, waiting for transfers between devices: 52.9 us -> none  [the longest x1 33.9 us: body(): lax.psum(head_part.astype(jnp.bfloat16), 'tp').astype(jnp.float32)]
    pallas_call x0 -> x5, Pallas kernels: none -> 50.6 us  [the longest x4 39.6 us: call_comm(): pl.pallas_call(kernel, out_shape=[jax.ShapeDtypeStruct(shape, dtype) for...]
    all_gather x1 -> x0, blocking collectives: 30.7 us -> none  [body(): portion = lax.all_gather(normed_mine, 'ep', axis=0, tiled=True)]
    unnamed x35 -> x33, local copies, waits for them, and re-layouts: 24.9 us -> 9.61 us
    dot_general x13 -> x5, matrix products: 16.8 us -> 1.59 us  [the longest x1 0.77 us: body(): jnp.dot(combine_table, returned.astype(F32), precision=lax.Precision.HIGH...]
    all_to_all x2 -> x0, waiting for transfers between devices: 13.7 us -> none  [the longest x1 6.88 us: body(): lax.all_to_all(outgoing, 'ep', split_axis=0, concat_axis=0, tiled=True)]
    all_to_all x2 -> x0, starting transfers between devices: 10.9 us -> none  [the longest x1 5.51 us: body(): lax.all_to_all(summed, 'ep', split_axis=0, concat_axis=0, tiled=True)]
  transfers between devices with their start and end apart: 6 -> 0, of which waited for: 6 -> 0; matrix products, arithmetic and copies ran while one was open for 5% -> 0% of each run, Pallas kernels for 0% -> 0%
where the time goes in v1:
time: 70.7 us; the launch traced here: 70.2 us
  Pallas kernels  50.6 us (72%)
  local copies, waits for them, and re-layouts  11.2 us (16%)
  matrix products  6.97 us (10%)
  other arithmetic  1.2 us (2%)
    pallas_call x4, Pallas kernels, call_comm(): pl.pallas_call(kernel, out_shape=[jax.ShapeDtypeStruct(shape, dtype) for...  39.6 us
    pallas_call x1, Pallas kernels, attention(): pl.pallas_call(functools.partial(attend_kernel, batch), grid=(seqs // bat...  11 us
    unnamed x33, local copies, waits for them, and re-layouts  9.61 us
    dot_general x1, matrix products, body(): jnp.einsum('nesf,efd->nesd', hidden, expert_down, preferred_element_type=...  4.73 us

profile of v1, /device:TPU:0, one launch (start us, length us, event | category | flops | bytes accessed | tf_op | source)
XLA Modules:
  0.0 70.2 jit_solution(8166164762433808696)
XLA Ops:
  0.0 0.8 %copy.43 = s32[16,2]{1,0:T(8,128)S(1)} copy(s32[16,2]{0,1:T(2,128)} %param.37) | data formatting | bytes 256 | tf_op args[14]
  0.8 0.7 broadcast_multiply_fusion
  2.3 0.8 %copy.42.bias_ref = f32[4,1]{1,0:T(4,128)S(1)} copy(f32[4,1]{0,1:T(1,128)} %bitcast.91) | data formatting | bytes 32 | tf_op jit(solution)/shard_map/broadcast_in_dim | solution.py:116
  3.0 1.2 %copy-done.1 = bf16[2048,256]{1,0:T(8,128)(2,1)S(1)} copy-done((bf16[2048,256]{1,0:T(8,128)(2,1)S(1)}, bf16[2048,256]{1,0:T(8,128)(2,1)}, u32[]{:S(2)}) %copy-start.1) | copy-done | bytes 1048600
  4.3 1.2 %copy-done.2 = bf16[2048,256]{1,0:T(8,128)(2,1)S(1)} copy-done((bf16[2048,256]{1,0:T(8,128)(2,1)S(1)}, bf16[2048,256]{1,0:T(8,128)(2,1)}, u32[]{:S(2)}) %copy-start.2) | copy-done | bytes 1048600
  5.5 1.2 %copy-done.3 = bf16[2048,256]{1,0:T(8,128)(2,1)S(1)} copy-done((bf16[2048,256]{1,0:T(8,128)(2,1)S(1)}, bf16[2048,256]{1,0:T(8,128)(2,1)}, u32[]{:S(2)}) %copy-start.3) | copy-done | bytes 1048600
  6.7 1.2 %copy-done.4 = bf16[256,2048]{1,0:T(8,128)(2,1)S(1)} copy-done((bf16[256,2048]{1,0:T(8,128)(2,1)S(1)}, bf16[256,2048]{1,0:T(8,128)(2,1)}, u32[]{:S(2)}) %copy-start.4) | copy-done | bytes 1048600
  7.9 0.8 %copy-done.5 = bf16[16,2048]{1,0:T(8,128)(2,1)S(1)} copy-done((bf16[16,2048]{1,0:T(8,128)(2,1)S(1)}, bf16[16,2048]{1,0:T(8,128)(2,1)}, u32[]{:S(2)}) %copy-start.5) | copy-done | bytes 65560
  8.8 0.9 %copy-done.6 = f32[16,4,1024]{2,1,0:T(4,128)S(1)} copy-done((f32[16,4,1024]{2,1,0:T(4,128)S(1)}, f32[16,4,1024]{2,1,0:T(4,128)}, u32[]{:S(2)}) %copy-start.6) | copy-done | bytes 262168
  9.7 0.7 %copy-done.7 = bf16[2048,4]{0,1:T(4,128)(2,1)S(1)} copy-done((bf16[2048,4]{0,1:T(4,128)(2,1)S(1)}, bf16[2048,4]{0,1:T(4,128)(2,1)}, u32[]{:S(2)}) %copy-start.7) | copy-done | bytes 16408
  10.4 0.7 copy-done.8
  11.1 0.7 copy-done.10
  11.8 11.0 %attend.1.part_ref = bf16[16,2048]{1,0:T(8,128)(2,1)S(1)} custom-call(s32[16]{0:T(128)S(1)} %copy-done.10, bf16[16,2048]{1,0:T(8,128)(2,1)S(1)} %copy-done.5, f32[1,2048]{1,0:T(1,128)S(1)} %bitcast.87, bf16[2048,256]{1,0:T(8,128)(2,1)S(1)} %copy-done.1, bf16[2048,256]{1,0:T(8,128)(2,1)S(1)} %copy-done.2, bf16[2048,256]{1,0:T(8,128)(2,1)S(1)} %copy-done.3, ...), custom_call_target="tpu_custom_call" | custom-call | tf_op jit(solution)/shard_map/attend/pallas_call | solution.py:85
  22.8 6.4 %comm_1.1 = (f32[16,2048]{1,0:T(8,128)S(1)}, bf16[16,2048]{1,0:T(8,128)(2,1)S(1)}, bf16[64,2048]{1,0:T(8,128)(2,1)S(1)}) custom-call(bf16[16,2048]{1,0:T(8,128)(2,1)S(1)} %attend.1.part_ref, bf16[16,2048]{1,0:T(8,128)(2,1)S(1)} %copy-done.5, f32[1,2048]{1,0:T(1,128)S(1)} %bitcast.88, bf16[64,16]{1,0:T(8,128)(2,1)S(1)} %copy.45.table_ref), custom_call_target="tpu_custom_call" | custom-call | tf_op jit(solution)/shard_map/comm_1/pallas_call | solution.py:261
  29.2 12.6 %comm_2.1 = (bf16[8,8,2048]{2,1,0:T(8,128)(2,1)S(1)}, bf16[8,16,512]{2,1,0:T(8,128)(2,1)S(1)}) custom-call(bf16[8,8,2048]{2,1,0:T(8,128)(2,1)S(1)} %bitcast.83, bf16[16,2048]{1,0:T(8,128)(2,1)S(1)} %get-tuple-element.16.norm_ref), custom_call_target="tpu_custom_call" | custom-call | tf_op jit(solution)/shard_map/comm_2/pallas_call | solution.py:261
  41.9 0.7 fusion.12
  42.6 4.7 %fusion.9 = bf16[8,4,2,2048]{3,0,2,1:T(8,128)(2,1)S(1)} fusion(bf16[4,256,2048]{2,1,0:T(8,128)(2,1)} %param.41, bf16[8,4,2,2048]{3,0,2,1:T(8,128)(2,1)S(1)} %bitcast.90, bf16[4,2048,256]{2,1,0:T(8,128)(2,1)} %param.40, f32[8,4,2,256]{3,0,2,1:T(8,128)S(1)} %fusion.12), kind=kOutput, calls=%fused_computation.7 | convolution fusion | flops 134447104 | bytes 8978432 | tf_op jit(solution)/shard_map/nesf,efd->nesd/dot_general | solution.py:351
  47.4 0.3 copy.49
  47.8 0.2 convolution_convert_fusion.2
  48.0 0.2 convolution_convert_fusion.1
  48.2 9.9 %comm_3.1 = (bf16[4,32,512]{2,1,0:T(8,128)(2,1)S(1)}, bf16[64,512]{1,0:T(8,128)(2,1)S(1)}) custom-call(bf16[4,32,512]{2,1,0:T(8,128)(2,1)S(1)} %bitcast.81, bf16[4,32,512]{2,1,0:T(8,128)(2,1)S(1)} %bitcast.82, bf16[64,2048]{1,0:T(8,128)(2,1)S(1)} %reshape.54.moe_ref), custom_call_target="tpu_custom_call" | custom-call | tf_op jit(solution)/shard_map/comm_3/pallas_call | solution.py:261
  58.1 0.2 convolution_convert_fusion
  58.4 10.8 %comm_4.1 = (f32[16,512]{1,0:T(8,128)S(1)}, bf16[8,8,512]{2,1,0:T(8,128)(2,1)S(1)}) custom-call(bf16[8,16,512]{2,1,0:T(8,128)(2,1)S(1)} %bitcast.78, bf16[8,8,512]{2,1,0:T(8,128)(2,1)S(1)} %bitcast.85), custom_call_target="tpu_custom_call" | custom-call | tf_op jit(solution)/shard_map/comm_4/pallas_call | solution.py:261
  69.4 0.8 %fusion.25 = bf16[16,512]{1,0:T(8,128)(2,1)} fusion(f32[16,64]{1,0:T(8,128)S(1)} %select_reduce_fusion, bf16[8,8,512]{2,1,0:T(8,128)(2,1)S(1)} %get-tuple-element.21, f32[16,512]{1,0:T(8,128)S(1)} %get-tuple-element.22, f32[16,2048]{1,0:T(8,128)S(1)} %get-tuple-element.14, s32[]{:T(128)S(6)} %select_n.7, f32[16]{0:T(128)S(1)} %fusion.29), kind=kOutput, calls=%fused_computation.17 | convolution fusion | flops 6324224 | bytes 151620 | tf_op jit(solution)/shard_map/dot_general | solution.py:388
  (36 shorter events, 1.3 us)
Async XLA Ops:
  0.0 47.7 %copy-start = (bf16[512,512]{1,0:T(8,128)(2,1)S(1)}, bf16[512,512]{1,0:T(8,128)(2,1)}, u32[]{:S(2)}) copy-start(bf16[512,512]{1,0:T(8,128)(2,1)} %param.42) | copy-start | bytes 1572868
  3.0 1.2 %copy-start.1 = (bf16[2048,256]{1,0:T(8,128)(2,1)S(1)}, bf16[2048,256]{1,0:T(8,128)(2,1)}, u32[]{:S(2)}) copy-start(bf16[2048,256]{1,0:T(8,128)(2,1)} %wq_ref.1) | copy-start | bytes 3145732
  4.2 1.2 %copy-start.2 = (bf16[2048,256]{1,0:T(8,128)(2,1)S(1)}, bf16[2048,256]{1,0:T(8,128)(2,1)}, u32[]{:S(2)}) copy-start(bf16[2048,256]{1,0:T(8,128)(2,1)} %wk_ref.1) | copy-start | bytes 3145732
  5.5 1.2 %copy-start.3 = (bf16[2048,256]{1,0:T(8,128)(2,1)S(1)}, bf16[2048,256]{1,0:T(8,128)(2,1)}, u32[]{:S(2)}) copy-start(bf16[2048,256]{1,0:T(8,128)(2,1)} %wv_ref.1) | copy-start | bytes 3145732
  6.7 1.2 %copy-start.4 = (bf16[256,2048]{1,0:T(8,128)(2,1)S(1)}, bf16[256,2048]{1,0:T(8,128)(2,1)}, u32[]{:S(2)}) copy-start(bf16[256,2048]{1,0:T(8,128)(2,1)} %wo_ref.1) | copy-start | bytes 3145732
  7.9 0.8 %copy-start.5 = (bf16[16,2048]{1,0:T(8,128)(2,1)S(1)}, bf16[16,2048]{1,0:T(8,128)(2,1)}, u32[]{:S(2)}) copy-start(bf16[16,2048]{1,0:T(8,128)(2,1)} %tok_ref.3) | copy-start | bytes 196612
  8.8 0.9 %copy-start.6 = (f32[16,4,1024]{2,1,0:T(4,128)S(1)}, f32[16,4,1024]{2,1,0:T(4,128)}, u32[]{:S(2)}) copy-start(f32[16,4,1024]{2,1,0:T(4,128)} %gate_ref.1) | copy-start | bytes 786436
  9.7 0.7 %copy-start.7 = (bf16[2048,4]{0,1:T(4,128)(2,1)S(1)}, bf16[2048,4]{0,1:T(4,128)(2,1)}, u32[]{:S(2)}) copy-start(bf16[2048,4]{0,1:T(4,128)(2,1)} %param.28) | copy-start | bytes 49156
  10.4 0.7 copy-start.8
  11.1 0.7 copy-start.10
  11.8 11.0 %copy-start.9 = (f32[2048]{0:T(1024)S(1)}, f32[2048]{0:T(1024)}, u32[]{:S(2)}) copy-start(f32[2048]{0:T(1024)} %param.35) | copy-start | bytes 24580
  11.8 30.2 %copy-start.11 = (bf16[4,2048,256]{2,1,0:T(8,128)(2,1)S(1)}, bf16[4,2048,256]{2,1,0:T(8,128)(2,1)}, u32[]{:S(2)}) copy-start(bf16[4,2048,256]{2,1,0:T(8,128)(2,1)} %param.39) | copy-start | bytes 12582916
  42.6 5.4 %copy-start.12 = (bf16[512,512]{1,0:T(8,128)(2,1)S(1)}, bf16[512,512]{1,0:T(8,128)(2,1)}, u32[]{:S(2)}) copy-start(bf16[512,512]{1,0:T(8,128)(2,1)} %param.43) | copy-start | bytes 1572868
  42.6 15.5 %copy-start.13 = (bf16[512,512]{1,0:T(8,128)(2,1)S(1)}, bf16[512,512]{1,0:T(8,128)(2,1)}, u32[]{:S(2)}) copy-start(bf16[512,512]{1,0:T(8,128)(2,1)} %param.44) | copy-start | bytes 1572868
  42.6 26.5 %copy-start.15 = (f32[2048]{0:T(1024)S(1)}, f32[2048]{0:T(1024)}, u32[]{:S(2)}) copy-start(f32[2048]{0:T(1024)} %param.45) | copy-start | bytes 24580
  47.3 21.9 %copy-start.14 = (f32[16,2]{0,1:T(2,128)S(1)}, f32[16,2]{0,1:T(2,128)}, u32[]{:S(2)}) copy-start(f32[16,2]{0,1:T(2,128)} %param.38) | copy-start | bytes 388
